TPU v7x, 512 devices: a whole 4x4x16 slice. The times are simulated.
512 devices in a mesh: sp: 32 (over z, core), tp: 16 (over y, x).
Axes of the slice: x: 4, y: 4, z: 16, core: 2. Of those that a mesh axis runs over, the one named last changes fastest.
Arguments:
- stream: bfloat16 [2048, 4096], P('tp', 'sp')
- values_in: bfloat16 [1024, 4096], P('tp', 'sp'), may hold values from -6 to 6
- in_gate: bfloat16 [1024, 4096], P('tp', 'sp'), may hold values from -6 to 6
- out_gate: bfloat16 [1024, 4096], P('tp', 'sp'), may hold values from -6 to 6
- documents: int32 [4096], P('sp'), may hold values from 0 to 63, never falling along the last dimension, each value on 1 to 256 neighbouring positions
- conv_taps: float32 [3, 1024], P(None, 'tp'), may hold values from -3.5 to 3.5
- head_gain: float32 [1024], P('tp'), may hold values from 0.1 to 1.9
- mix_weight: bfloat16 [1024, 2048], P('tp'), may hold values from -0.25 to 0.25
- norm_gain: float32 [2048], P('tp'), may hold values from 0.1 to 1.9
- routes: int32 [4096, 4], P('sp'), may hold values from 0 to 31, all different within a row; in each aligned block of 128 rows (0 to 127, 128 to 255, ...) at most 24 rows name the same one
- route_weight: float32 [4096, 4], P('sp'), may hold values from 0.2 to 1
- expert_gate: bfloat16 [32, 2048, 2048], P('sp', None, 'tp'), may hold values from -0.125 to 0.125
- expert_up: bfloat16 [32, 2048, 2048], P('sp', None, 'tp'), may hold values from -0.125 to 0.125
- expert_down: bfloat16 [32, 2048, 2048], P('sp', None, 'tp'), may hold values from -0.125 to 0.125
- shared_gate: bfloat16 [2048, 2048], P(None, 'tp'), may hold values from -0.125 to 0.125
- shared_up: bfloat16 [2048, 2048], P(None, 'tp'), may hold values from -0.125 to 0.125
- shared_down: bfloat16 [2048, 2048], P('tp'), may hold values from -0.1875 to 0.1875
Outputs:
- layer_out: bfloat16 [2048, 4096], P('tp', 'sp')
Inputs may be any that keep to these rules, and one draw needn't show every extreme that they name: `routes`: each row names 4 different experts. In each aligned block of 128 rows no expert is named by more than 24 rows, a bound that some block reaches. `documents`: document numbers never fall along the positions; each document has 1 to 256 positions, and one has exactly that many.
All inputs are finite; a program needn't handle non-finite values.
Results may differ from a plain program's by a relative error of at most 0.015.
Values may be sent and summed in bfloat16 or wider, within the bound.
No kernel may reach another device: no remote copies, remote signals or barrier semaphores. Data moves between devices by JAX's collectives and lax.ppermute only.
A program may use at most 64 MiB of HBM per device.

v0:
```python
import jax
import jax.numpy as jnp
from jax import lax
from jax.sharding import Mesh
from jax.sharding import PartitionSpec as P

D = 2048
HEAD = 64
TP = ("tp_0", "tp_1")


epsilon = 1e-06


def from_behind(x, axis, by):
    size = lax.axis_size(axis)
    pairs = [(i, i + by) for i in range(size) if 0 <= i + by < size]
    return lax.ppermute(x, axis, pairs)


def in_blocks(x, dim, size):
    before, after = (x.shape[:dim], x.shape[dim + 1 :])
    return jnp.moveaxis(x.reshape(*before, size, -1, *after), dim, 0)


def sum_at_owner(x, axis, dim):
    pieces = in_blocks(x, dim, lax.axis_size(axis))
    arrived = lax.all_to_all(pieces, axis, split_axis=0, concat_axis=0, tiled=True)
    return arrived.astype(jnp.float32).sum(axis=0)


def from_everyone(x, axis):
    size = lax.axis_size(axis)
    return lax.all_to_all(jnp.broadcast_to(x[None], (size, *x.shape)), axis, 0, 0, tiled=True)


def taken_together(x, axis):
    everything = from_everyone(x, axis)
    return jnp.sum(everything, axis=0)


def joined_along(pieces, dim):
    pieces = jnp.moveaxis(pieces, 0, dim)
    shape = pieces.shape
    return pieces.reshape(*shape[:dim], shape[dim] * shape[dim + 1], *shape[dim + 2 :])


def gather_directly(x, axis, dim):
    pieces = from_everyone(x, axis)
    return joined_along(pieces, dim)


def gather_axes(x, axes, dim):
    if not axes:
        return x
    nearer = lax.all_gather(x, axes[-1], axis=dim, tiled=True)
    return gather_axes(nearer, axes[:-1], dim)


def contract_rows(left, right):
    return lax.dot_general(
        left, right, (((0,), (0,)), ((), ())), preferred_element_type=jnp.float32
    )


def local(
    stream,
    values_in,
    in_gate,
    out_gate,
    documents,
    conv_taps,
    head_gain,
    mix_weight,
    norm_gain,
    routes,
    route_weight,
    expert_gate,
    expert_up,
    expert_down,
    shared_gate,
    shared_up,
    shared_down,
):
    positions = stream.shape[1]
    feat_rows = stream.shape[0]
    sp_count = lax.axis_size("sp")
    top_count = routes.shape[1]
    capacity = 3 * positions * top_count // (2 * sp_count)
    slot_total = sp_count * capacity
    tails = jnp.stack([values_in[:, -2:], in_gate[:, -2:]])
    before, before_docs = from_behind((tails, documents[-2:]), "sp", 1)
    joined = jnp.concatenate([before, jnp.stack([values_in, in_gate])], axis=2).astype(jnp.float32)
    product = joined[0] * joined[1]
    doc_ids = jnp.concatenate([before_docs, documents])
    convolved = jnp.zeros((values_in.shape[0], positions), jnp.float32)
    for offset in range(3):
        same_doc = (doc_ids[offset : offset + positions] == documents).astype(jnp.float32)
        convolved = (
            convolved
            + conv_taps[offset][:, None]
            * product[:, offset : offset + positions]
            * same_doc[None, :]
        )
    mixed = out_gate.astype(jnp.float32) * convolved
    heads = mixed.reshape(-1, HEAD, positions)
    heads = heads * lax.rsqrt(jnp.mean(heads * heads, axis=1, keepdims=True) + epsilon)
    normed_heads = (heads.reshape(mixed.shape) * head_gain[:, None]).astype(jnp.bfloat16)
    mixer = sum_at_owner(contract_rows(mix_weight, normed_heads).astype(jnp.bfloat16), TP, 0)
    hidden_state = stream.astype(jnp.float32) + mixer
    squares = taken_together(jnp.sum(hidden_state * hidden_state, axis=0), TP)
    normed = (hidden_state * lax.rsqrt(squares / D + epsilon)[None, :] * norm_gain[:, None]).astype(
        jnp.bfloat16
    )
    full_rows = gather_directly(normed, TP, 0)
    shared_mid = (
        jax.nn.silu(contract_rows(shared_gate, full_rows)) * contract_rows(shared_up, full_rows)
    ).astype(jnp.bfloat16)
    shared = sum_at_owner(contract_rows(shared_down, shared_mid).astype(jnp.bfloat16), TP, 0)
    flat_routes = routes.reshape(-1)
    onehot = (flat_routes[:, None] == jnp.arange(sp_count, dtype=jnp.int32)[None, :]).astype(
        jnp.int32
    )
    earlier = jnp.cumsum(onehot, axis=0) - onehot
    slot = jnp.sum(earlier * onehot, axis=1)
    column = flat_routes * capacity + slot
    chosen = (column[:, None] == jnp.arange(slot_total, dtype=jnp.int32)[None, :]).reshape(
        positions, top_count, slot_total
    )
    dispatch = jnp.any(chosen, axis=1).astype(jnp.bfloat16)
    combine = jnp.sum(chosen.astype(jnp.float32) * route_weight[:, :, None], axis=1)
    sent = jnp.dot(normed, dispatch, preferred_element_type=jnp.float32).astype(jnp.bfloat16)
    arrived = lax.all_to_all(
        sent.reshape(feat_rows, sp_count, capacity), "sp", split_axis=1, concat_axis=1, tiled=True
    )
    block_rows = gather_axes(arrived.reshape(feat_rows, slot_total), TP, 0)
    gate_rows = expert_gate[0]
    up_rows = expert_up[0]
    gate = contract_rows(gate_rows, block_rows)
    upward = contract_rows(up_rows, block_rows)
    expert_mid = (jax.nn.silu(gate) * upward).astype(jnp.bfloat16)
    weight_rows = expert_down[0]
    summed = contract_rows(weight_rows, lax.all_gather(expert_mid, TP, axis=0, tiled=True)).astype(
        jnp.bfloat16
    )
    returned = lax.all_to_all(
        summed.reshape(feat_rows, sp_count, capacity), "sp", split_axis=1, concat_axis=1, tiled=True
    )
    routed = lax.dot_general(
        returned.reshape(feat_rows, slot_total).astype(jnp.float32),
        combine,
        (((1,), (1,)), ((), ())),
        precision=lax.Precision.HIGHEST,
        preferred_element_type=jnp.float32,
    )
    return (hidden_state + shared + routed).astype(jnp.bfloat16)


def solution(mesh):
    split = Mesh(mesh.devices.reshape(mesh.shape["sp"], 4, 4), ("sp", "tp_0", "tp_1"))
    in_specs = (
        P(TP, "sp"),
        P(TP, "sp"),
        P(TP, "sp"),
        P(TP, "sp"),
        P("sp"),
        P(None, TP),
        P(TP),
        P(TP, None),
        P(TP),
        P("sp", None),
        P("sp", None),
        P("sp", None, TP),
        P("sp", None, TP),
        P("sp", None, TP),
        P(None, TP),
        P(None, TP),
        P(TP, None),
    )
    out_specs = P(TP, "sp")
    return jax.shard_map(local, mesh=split, in_specs=in_specs, out_specs=out_specs, check_vma=False)
```

profile of v0, /device:TPU:1, one launch (start us, length us, event | category | flops | bytes accessed | tf_op | source)
XLA Modules:
  0.0 260.6 jit_solution(9237096032666451016)
XLA Ops:
  6.5 0.8 slice.51
  7.3 4.9 %collective-permute-start.1 = (s32[2]{0:T(128)S(1)}, s32[2]{0:T(128)S(1)}, u32[]{:S(2)}, u32[]{:S(2)}) collective-permute-start(s32[2]{0:T(128)S(1)} %slice.51), channel_id=1, source_target_pairs={{0,16},{16,32},{32,48},{48,64},{64,80},{80,96},{96,112},{112,128},... | collective-permute-start | bytes 32 | tf_op jit(solution)/shard_map/ppermute | solution.py:18
  12.2 0.8 slice.46
  13.0 0.1 copy.82
  13.1 0.8 slice.47
  14.0 1.9 collective-permute-start
  16.0 0.8 slice_bitcast_fusion.2
  16.8 0.8 copy.92
  17.6 0.1 eq.51
  17.7 0.7 pad_add_fusion
  18.4 0.7 compare_convert_fusion.1
  19.2 0.1 copy.84
  19.3 0.8 maximum_convert_fusion
  20.1 0.8 multiply_reduce_fusion.1
  21.0 1.4 fusion.1
  22.4 0.9 copy.106
  23.3 6.7 %all-to-all-start = ((bf16[16,128,128]{1,2,0:T(8,128)(2,1)}), bf16[16,128,128]{1,2,0:T(8,128)(2,1)S(1)}, u32[]{:S(2)}, u32[]{:S(2)}) async-start(bf16[16,128,128]{1,2,0:T(8,128)(2,1)} %bitcast.90), calls=%async_computation | async-start | bytes 1048576 | tf_op jit(solution)/shard_map/all_to_all | solution.py:28
  30.0 0.1 eq.47
  30.1 1.2 reduce-window.6
  31.3 0.2 slice_reduce_fusion
  31.6 0.1 fusion.13
  31.7 0.1 reduce_sum.71
  31.9 8.8 %all-to-all-done = bf16[16,128,128]{1,2,0:T(8,128)(2,1)S(1)} async-done(((bf16[16,128,128]{1,2,0:T(8,128)(2,1)}), bf16[16,128,128]{1,2,0:T(8,128)(2,1)S(1)}, u32[]{:S(2)}, u32[]{:S(2)}) %all-to-all-start) | async-done | bytes 524320 | tf_op jit(solution)/shard_map/all_to_all | solution.py:28
  40.7 0.1 copy.87
  40.8 0.6 broadcast_in_dim.4
  41.5 3.5 %all-to-all-start.1 = ((f32[16,1,128]{2,1,0:T(1,128)}), f32[16,1,128]{2,1,0:T(1,128)S(1)}, u32[]{:S(2)}, u32[]{:S(2)}) async-start(f32[16,1,128]{2,1,0:T(1,128)} %broadcast_in_dim.4), calls=%async_computation.1 | async-start | bytes 16384 | tf_op jit(solution)/shard_map/all_to_all | solution.py:34
  45.0 0.3 fusion
  45.3 6.0 %all-to-all-done.1 = f32[16,1,128]{2,1,0:T(1,128)S(1)} async-done(((f32[16,1,128]{2,1,0:T(1,128)}), f32[16,1,128]{2,1,0:T(1,128)S(1)}, u32[]{:S(2)}, u32[]{:S(2)}) %all-to-all-start.1) | async-done | bytes 8224 | tf_op jit(solution)/shard_map/all_to_all | solution.py:34
  51.4 0.2 convolution_convert_fusion.3
  51.6 0.2 copy.96
  51.8 35.9 %all_to_all.31 = bf16[128,32,24]{0,2,1:T(8,128)(2,1)S(1)} all-to-all(bf16[128,32,24]{0,2,1:T(8,128)(2,1)S(1)} %bitcast.93), channel_id=1, replica_groups=mesh['sp'=32,'tp_0'=4,'tp_1'=4] {'sp'}, dimensions={1} | all-to-all | bytes 393216 | tf_op jit(solution)/shard_map/all_to_all | solution.py:133
  87.7 15.4 %all_gather.9 = bf16[512,768]{0,1:T(8,128)(2,1)} all-gather(bf16[128,768]{0,1:T(8,128)(2,1)S(1)} %bitcast.95), channel_id=1, replica_groups=mesh['sp'=32,'tp_0'=4,'tp_1'=4] {'tp_1'}, dimensions={0}, use_global_device_ids=true | all-gather | bytes 983040 | tf_op jit(solution)/shard_map/all_gather | solution.py:56
  103.2 37.7 %all-gather.3.cloned.1.call-done = bf16[2048,768]{0,1:T(8,128)(2,1)} async-done(((bf16[512,768]{0,1:T(8,128)(2,1)}), bf16[2048,768]{0,1:T(8,128)(2,1)}) %all-gather.3.cloned.1.call-update) | async-done | bytes 3145744 | tf_op jit(solution)/shard_map/all_gather | solution.py:56
  140.8 3.0 %convolution_bitcast_fusion.1 = f32[128,768]{0,1:T(8,128)S(1)} fusion(bf16[2048,768]{0,1:T(8,128)(2,1)} %all-gather.3.cloned.1.call-done, bf16[1,2048,128]{2,1,0:T(8,128)(2,1)S(1)} %copy-done.2), kind=kOutput, calls=%fused_computation.8 | convolution fusion | flops 402653184 | bytes 4063232 | tf_op jit(solution)/shard_map/dot_general | solution.py:61
  143.9 1.7 fusion.4
  145.6 0.1 broadcast_in_dim.5
  145.7 15.9 %all_to_all.32 = bf16[16,128,128]{2,1,0:T(8,128)(2,1)S(1)} all-to-all(bf16[16,128,128]{2,1,0:T(8,128)(2,1)S(1)} %broadcast_in_dim.5), channel_id=1, replica_groups=mesh['sp'=32,'tp_0'=4,'tp_1'=4] {'tp_0','tp_1'}, dimensions={0} | all-to-all | bytes 1048576 | tf_op jit(solution)/shard_map/all_to_all | solution.py:34
  161.6 0.3 convolution_bitcast_fusion.3
  162.0 0.6 fusion.2
  162.6 0.9 copy.105
  163.5 3.7 %all-to-all-start.3 = ((bf16[16,128,128]{1,2,0:T(8,128)(2,1)}), bf16[16,128,128]{1,2,0:T(8,128)(2,1)S(1)}, u32[]{:S(2)}, u32[]{:S(2)}) async-start(bf16[16,128,128]{1,2,0:T(8,128)(2,1)} %bitcast.89), calls=%async_computation.3 | async-start | bytes 1048576 | tf_op jit(solution)/shard_map/all_to_all | solution.py:28
  167.2 48.8 %all-gather.5.cloned.1.call-done = bf16[2048,768]{0,1:T(8,128)(2,1)} async-done(((bf16[128,768]{0,1:T(8,128)(2,1)}), bf16[2048,768]{0,1:T(8,128)(2,1)}) %all-gather.5.cloned.1.call-update) | async-done | bytes 3145744 | tf_op jit(solution)/shard_map/all_gather | solution.py:143
  216.0 3.6 %convolution_convert_fusion.2 = bf16[768,128]{1,0:T(8,128)(2,1)} fusion(bf16[2048,768]{0,1:T(8,128)(2,1)} %all-gather.5.cloned.1.call-done, bf16[1,2048,128]{2,1,0:T(8,128)(2,1)S(1)} %copy-done.10), kind=kOutput, calls=%fused_computation.11 | convolution fusion | flops 402751488 | bytes 3866624 | tf_op jit(solution)/shard_map/dot_general | solution.py:61
  219.6 14.4 %all-to-all-start.5 = ((bf16[128,32,24]{0,2,1:T(8,128)(2,1)}), bf16[128,32,24]{0,2,1:T(8,128)(2,1)S(1)}, u32[]{:S(2)}, u32[]{:S(2)}) async-start(bf16[128,32,24]{0,2,1:T(8,128)(2,1)} %bitcast.23), calls=%async_computation.5 | async-start | bytes 393216 | tf_op jit(solution)/shard_map/all_to_all | solution.py:146
  234.0 0.2 select_reduce_fusion
  234.3 0.1 copy.91
  234.4 18.4 %all-to-all-done.5 = bf16[128,32,24]{0,2,1:T(8,128)(2,1)S(1)} async-done(((bf16[128,32,24]{0,2,1:T(8,128)(2,1)}), bf16[128,32,24]{0,2,1:T(8,128)(2,1)S(1)}, u32[]{:S(2)}, u32[]{:S(2)}) %all-to-all-start.5) | async-done | bytes 196640 | tf_op jit(solution)/shard_map/all_to_all | solution.py:146
  252.8 1.0 fusion.6
  (44 shorter events, 0.7 us)
Async XLA Ops:
  6.5 155.4 %copy-start = (bf16[128,2048]{1,0:T(8,128)(2,1)S(1)}, bf16[128,2048]{1,0:T(8,128)(2,1)}, u32[]{:S(2)}) copy-start(bf16[128,2048]{1,0:T(8,128)(2,1)} %param.33) | copy-start | bytes 1572868
  6.5 25.3 %copy-start.6 = (s32[128,4]{0,1:T(4,128)S(1)}, s32[128,4]{0,1:T(4,128)}, u32[]{:S(2)}) copy-start(s32[128,4]{0,1:T(4,128)} %param.26) | copy-start | bytes 6148
  6.5 34.3 %copy-start.5 = (bf16[128,128]{1,0:T(8,128)(2,1)S(1)}, bf16[128,128]{1,0:T(8,128)(2,1)}, u32[]{:S(2)}) copy-start(bf16[128,128]{1,0:T(8,128)(2,1)} %param.17) | copy-start | bytes 98308
  6.5 44.8 %copy-start.8 = (f32[128]{0:T(128)S(1)}, f32[128]{0:T(128)}, u32[]{:S(2)}) copy-start(f32[128]{0:T(128)} %param.25) | copy-start | bytes 1540
  7.3 10.3 %collective-permute-start.1 = (s32[2]{0:T(128)S(1)}, s32[2]{0:T(128)S(1)}, u32[]{:S(2)}, u32[]{:S(2)}) collective-permute-start(s32[2]{0:T(128)S(1)} %slice.51), channel_id=1, source_target_pairs={{0,16},{16,32},{32,48},{48,64},{64,80},{80,96},{96,112},{112,128},... | collective-permute-start | bytes 32 | tf_op jit(solution)/shard_map/ppermute | solution.py:18
  14.0 5.1 %collective-permute-start = (bf16[2,64,2]{1,2,0:T(2,128)(2,1)S(1)}, bf16[2,64,2]{1,2,0:T(2,128)(2,1)S(1)}, u32[]{:S(2)}, u32[]{:S(2)}) collective-permute-start(bf16[2,64,2]{1,2,0:T(2,128)(2,1)S(1)} %pad_maximum_fusion), channel_id=1, source_target_pairs={{0,16},{16,32},{32,48},{48,64},{64,80},{80,96},{96,112},{112,128},... | collective-permute-start | bytes 1544 | tf_op jit(solution)/shard_map/ppermute | solution.py:18
  22.4 118.5 %copy-start.2 = (bf16[1,2048,128]{2,1,0:T(8,128)(2,1)S(1)}, bf16[1,2048,128]{2,1,0:T(8,128)(2,1)}, u32[]{:S(2)}) copy-start(bf16[1,2048,128]{2,1,0:T(8,128)(2,1)} %param.28) | copy-start | bytes 1572868
  23.3 17.3 %all-to-all-start = ((bf16[16,128,128]{1,2,0:T(8,128)(2,1)}), bf16[16,128,128]{1,2,0:T(8,128)(2,1)S(1)}, u32[]{:S(2)}, u32[]{:S(2)}) async-start(bf16[16,128,128]{1,2,0:T(8,128)(2,1)} %bitcast.90), calls=%async_computation | async-start | bytes 1048576 | tf_op jit(solution)/shard_map/all_to_all | solution.py:28
  41.5 9.8 %all-to-all-start.1 = ((f32[16,1,128]{2,1,0:T(1,128)}), f32[16,1,128]{2,1,0:T(1,128)S(1)}, u32[]{:S(2)}, u32[]{:S(2)}) async-start(f32[16,1,128]{2,1,0:T(1,128)} %broadcast_in_dim.4), calls=%async_computation.1 | async-start | bytes 16384 | tf_op jit(solution)/shard_map/all_to_all | solution.py:34
  44.9 95.9 %all-gather.3.cloned.1.call-start = ((), (), s32[]{:S(2)}) async-start(), calls=%async_computation.6 | async-start | bytes 3932160 | tf_op jit(solution)/shard_map/all_gather | solution.py:56
  103.1 40.8 %copy-start.9 = (bf16[1,2048,128]{2,1,0:T(8,128)(2,1)S(1)}, bf16[1,2048,128]{2,1,0:T(8,128)(2,1)}, u32[]{:S(2)}) copy-start(bf16[1,2048,128]{2,1,0:T(8,128)(2,1)} %param.29) | copy-start | bytes 1572868
  103.1 112.9 %all-gather.5.cloned.1.call-start = ((), (), s32[]{:S(2)}) async-start(), calls=%async_computation.7 | async-start | bytes 3342336 | tf_op jit(solution)/shard_map/all_gather | solution.py:143
  140.8 3.0 %copy-start.1 = (bf16[2048,768]{0,1:T(8,128)(2,1)S(1)}, bf16[2048,768]{0,1:T(8,128)(2,1)}, u32[]{:S(2)}) copy-start(bf16[2048,768]{0,1:T(8,128)(2,1)} %all-gather.3.cloned.1.call-done) | copy-start | bytes 9437188
  143.9 17.7 %copy-start.3 = (bf16[2048,128]{1,0:T(8,128)(2,1)S(1)}, bf16[2048,128]{1,0:T(8,128)(2,1)}, u32[]{:S(2)}) copy-start(bf16[2048,128]{1,0:T(8,128)(2,1)} %param.31) | copy-start | bytes 1572868
  145.6 16.4 %copy-start.4 = (bf16[2048,128]{1,0:T(8,128)(2,1)S(1)}, bf16[2048,128]{1,0:T(8,128)(2,1)}, u32[]{:S(2)}) copy-start(bf16[2048,128]{1,0:T(8,128)(2,1)} %param.32) | copy-start | bytes 1572868
  145.7 70.4 %copy-start.10 = (bf16[1,2048,128]{2,1,0:T(8,128)(2,1)S(1)}, bf16[1,2048,128]{2,1,0:T(8,128)(2,1)}, u32[]{:S(2)}) copy-start(bf16[1,2048,128]{2,1,0:T(8,128)(2,1)} %param.30) | copy-start | bytes 1572868
  163.5 70.5 %copy-start.7 = (f32[128,4]{0,1:T(4,128)S(1)}, f32[128,4]{0,1:T(4,128)}, u32[]{:S(2)}) copy-start(f32[128,4]{0,1:T(4,128)} %param.27) | copy-start | bytes 6148
  163.5 56.1 %all-to-all-start.3 = ((bf16[16,128,128]{1,2,0:T(8,128)(2,1)}), bf16[16,128,128]{1,2,0:T(8,128)(2,1)S(1)}, u32[]{:S(2)}, u32[]{:S(2)}) async-start(bf16[16,128,128]{1,2,0:T(8,128)(2,1)} %bitcast.89), calls=%async_computation.3 | async-start | bytes 1048576 | tf_op jit(solution)/shard_map/all_to_all | solution.py:28
  219.6 33.2 %all-to-all-start.5 = ((bf16[128,32,24]{0,2,1:T(8,128)(2,1)}), bf16[128,32,24]{0,2,1:T(8,128)(2,1)S(1)}, u32[]{:S(2)}, u32[]{:S(2)}) async-start(bf16[128,32,24]{0,2,1:T(8,128)(2,1)} %bitcast.23), calls=%async_computation.5 | async-start | bytes 393216 | tf_op jit(solution)/shard_map/all_to_all | solution.py:146
Sparse Core Ops, SparseCore 0:
  103.2 37.5 all-gather.2
  145.7 70.2 all-gather.4
where the time goes:
time: 262 us; the launch traced here: 261 us
  waiting for transfers between devices  120 us (46%)
  blocking collectives  67.2 us (26%)
  starting transfers between devices  35.2 us (13%)
  between operations  13.7 us (5%)
  matrix products  11.7 us (4%)
  local copies, waits for them, and re-layouts  7.81 us (3%)
  other arithmetic  5.27 us (2%)
    all_gather x1, waiting for transfers between devices, local(): lax.all_gather(expert_mid, TP, axis=0, tiled=True)  48.8 us
    all_gather x1, waiting for transfers between devices, gather_axes(): nearer = lax.all_gather(x, axes[-1], axis=dim, tiled=True)  37.7 us
    all_to_all x1, blocking collectives, local(): lax.all_to_all(sent.reshape(feat_rows, sp_count, capacity), 'sp', split_a...  35.9 us
    all_to_all x1, waiting for transfers between devices, local(): lax.all_to_all(summed.reshape(feat_rows, sp_count, capacity), 'sp', split...  18.4 us
    all_to_all x1, blocking collectives, from_everyone(): lax.all_to_all(jnp.broadcast_to(x[None], (size, *x.shape)), axis, 0, 0, t...  15.9 us
    all_gather x1, blocking collectives, gather_axes(): nearer = lax.all_gather(x, axes[-1], axis=dim, tiled=True)  15.4 us
    all_to_all x1, starting transfers between devices, local(): lax.all_to_all(summed.reshape(feat_rows, sp_count, capacity), 'sp', split...  14.4 us
    dot_general x6, matrix products, contract_rows(): lax.dot_general(left, right, (((0,), (0,)), ((), ())), preferred_element_...  10.5 us
  transfers between devices with their start and end apart: 8, of which 5 were waited for; matrix products, arithmetic and copies ran while one was open for 5% of the time, Pallas kernels for 0%

commit v1 on v0

v1 whole, which is shorter than its diff:
```python
import jax
import jax.numpy as jnp
from jax import lax
from jax.sharding import Mesh
from jax.sharding import PartitionSpec as P

D = 2048
HEAD = 64
TP = ("ty", "tx")


epsilon = 1e-06


def shifted(x, axis, by, wrap):
    size = lax.axis_size(axis)
    pairs = [(i, (i + by) % size) for i in range(size) if wrap or 0 <= i + by < size]
    return lax.ppermute(x, axis, pairs)


def sum_at_owner(x, axis):
    pieces = x.reshape(lax.axis_size(axis), -1, x.shape[-1])
    arrived = lax.all_to_all(pieces, axis, split_axis=0, concat_axis=0, tiled=True)
    return arrived.astype(jnp.float32).sum(axis=0)


def from_everyone(x, axis):
    size = lax.axis_size(axis)
    return lax.all_to_all(jnp.broadcast_to(x[None], (size, *x.shape)), axis, 0, 0, tiled=True)


def contract_rows(left, right):
    return lax.dot_general(
        left, right, (((0,), (0,)), ((), ())), preferred_element_type=jnp.float32
    )


def three_terms(x):
    high = x.astype(jnp.bfloat16)
    rest = x - high.astype(jnp.float32)
    middle = rest.astype(jnp.bfloat16)
    low = (rest - middle.astype(jnp.float32)).astype(jnp.bfloat16)
    return [high, middle, low]


def local(
    stream,
    values_in,
    in_gate,
    out_gate,
    documents,
    conv_taps,
    head_gain,
    mix_weight,
    norm_gain,
    routes,
    route_weight,
    expert_gate,
    expert_up,
    expert_down,
    shared_gate,
    shared_up,
    shared_down,
):
    positions = stream.shape[1]
    feat_rows = stream.shape[0]
    sp_count = lax.axis_size("sp")
    parts = lax.axis_size("ty")
    top_count = routes.shape[1]
    capacity = 3 * positions * top_count // (2 * sp_count)
    share = capacity // parts
    row = lax.axis_index("ty")
    col = lax.axis_index("tx")

    packed = jnp.stack([expert_gate[0], expert_up[0], expert_down[0]])
    packed = packed.reshape(3, parts, 2, -1, feat_rows, feat_rows)
    packed = packed.transpose(2, 0, 3, 1, 4, 5).reshape(2, 3, D // 2, feat_rows)
    before_w = shifted(packed, "ty", 1, True)
    after_w = shifted(packed, "ty", -1, True)
    far_first = shifted(before_w[0], "ty", 1, True)
    far_second = shifted(after_w[1], "ty", -1, True)
    cycle = [
        (packed[0], packed[1]),
        (after_w[0], after_w[1]),
        (far_first, far_second),
        (before_w[0], before_w[1]),
    ]

    def in_order(blocks):
        twice = jnp.concatenate([blocks, blocks], axis=0)
        return lax.dynamic_slice_in_dim(twice, (parts - row) % parts, parts, axis=0)

    tails = jnp.stack([values_in[:, -2:], in_gate[:, -2:]])
    before, before_docs = shifted((tails, documents[-2:]), "sp", 1, False)
    joined = jnp.concatenate([before, jnp.stack([values_in, in_gate])], axis=2).astype(jnp.float32)
    product = joined[0] * joined[1]
    doc_ids = jnp.concatenate([before_docs, documents])
    convolved = jnp.zeros((values_in.shape[0], positions), jnp.float32)
    for offset in range(3):
        same_doc = (doc_ids[offset : offset + positions] == documents).astype(jnp.float32)
        convolved = (
            convolved
            + conv_taps[offset][:, None]
            * product[:, offset : offset + positions]
            * same_doc[None, :]
        )
    mixed = out_gate.astype(jnp.float32) * convolved
    heads = mixed.reshape(-1, HEAD, positions)
    heads = heads * lax.rsqrt(jnp.mean(heads * heads, axis=1, keepdims=True) + epsilon)
    normed_heads = (heads.reshape(mixed.shape) * head_gain[:, None]).astype(jnp.bfloat16)
    mixer = sum_at_owner(contract_rows(mix_weight, normed_heads).astype(jnp.bfloat16), TP)
    hidden_state = stream.astype(jnp.float32) + mixer

    squares = three_terms(jnp.sum(hidden_state * hidden_state, axis=0, keepdims=True))
    scaled = (hidden_state * norm_gain[:, None]).astype(jnp.bfloat16)
    filler = jnp.zeros((13, positions), jnp.bfloat16)
    everyone = from_everyone(jnp.concatenate([scaled, *squares, filler]), TP)
    total = jnp.sum(everyone[:, feat_rows : feat_rows + 3].astype(jnp.float32), axis=(0, 1))
    inverse = lax.rsqrt(total / D + epsilon)
    full_rows = (everyone[:, :feat_rows].astype(jnp.float32) * inverse).astype(jnp.bfloat16)

    flat_routes = routes.reshape(-1)
    onehot = (flat_routes[:, None] == jnp.arange(sp_count, dtype=jnp.int32)[None, :]).astype(
        jnp.int32
    )
    earlier = jnp.cumsum(onehot, axis=0) - onehot
    slot = jnp.sum(earlier * onehot, axis=1)
    inside = (slot >= row * share) & (slot < (row + 1) * share)
    column = jnp.where(inside, flat_routes * share + slot - row * share, -1)
    slot_total = sp_count * share
    chosen = (column[:, None] == jnp.arange(slot_total, dtype=jnp.int32)[None, :]).reshape(
        positions, top_count, slot_total
    )
    dispatch = jnp.any(chosen, axis=1).astype(jnp.bfloat16)
    combine = jnp.sum(chosen.astype(jnp.float32) * route_weight[:, :, None], axis=1)

    by_col = full_rows.reshape(parts, -1, feat_rows, positions)
    mine = lax.dynamic_index_in_dim(by_col, col, 1, keepdims=False)
    sent = lax.dot_general(
        dispatch,
        mine.reshape(parts * feat_rows, positions),
        (((0,), (1,)), ((), ())),
        preferred_element_type=jnp.float32,
    ).astype(jnp.bfloat16)
    arrived = lax.all_to_all(
        sent.reshape(sp_count, share * parts, feat_rows), "sp", split_axis=0, concat_axis=0, tiled=True
    )

    rows_full = full_rows.reshape(D, positions)
    shared_mid = (
        jax.nn.silu(contract_rows(shared_gate, rows_full)) * contract_rows(shared_up, rows_full)
    ).astype(jnp.bfloat16)
    shared = contract_rows(shared_down, shared_mid)

    def times(x, which, block):
        half = x.shape[0] // 2

        def part(k):
            w = cycle[block][k][which].reshape(half, -1, feat_rows)
            return lax.dot_general(
                x[k * half : (k + 1) * half],
                w,
                (((0, 2), (0, 1)), ((), ())),
                preferred_element_type=jnp.float32,
            )

        return part(0) + part(1)

    block_rows = lax.all_gather(arrived.reshape(slot_total, parts * feat_rows), "tx", axis=0)
    expert_mid = in_order(
        jnp.stack(
            [
                (jax.nn.silu(times(block_rows, 0, n)) * times(block_rows, 1, n)).astype(jnp.bfloat16)
                for n in range(parts)
            ]
        )
    )
    expert_mid = expert_mid.transpose(1, 0, 2).reshape(slot_total, parts * feat_rows)
    all_mid = lax.all_gather(expert_mid, "tx", axis=0)
    summed = in_order(
        jnp.stack([times(all_mid, 2, n).astype(jnp.bfloat16) for n in range(parts)])
    )
    summed = summed.transpose(1, 0, 2).reshape(sp_count, share * parts, feat_rows)
    returned = lax.all_to_all(summed, "sp", split_axis=0, concat_axis=0, tiled=True)
    routed = lax.dot_general(
        returned.reshape(slot_total, parts * feat_rows).astype(jnp.float32),
        combine,
        (((0,), (1,)), ((), ())),
        precision=lax.Precision.HIGHEST,
        preferred_element_type=jnp.float32,
    )
    here = (jnp.arange(lax.axis_size("tx")) == col).astype(jnp.float32)
    both = shared.reshape(parts, -1, feat_rows, positions) + (
        routed.reshape(parts, 1, feat_rows, positions) * here[None, :, None, None]
    )
    experts = sum_at_owner(both.reshape(D, positions).astype(jnp.bfloat16), TP)
    return (hidden_state + experts).astype(jnp.bfloat16)


def solution(mesh):
    split = Mesh(mesh.devices.reshape(mesh.shape["sp"], 4, 4), ("sp", "ty", "tx"))
    in_specs = (
        P(TP, "sp"),
        P(TP, "sp"),
        P(TP, "sp"),
        P(TP, "sp"),
        P("sp"),
        P(None, TP),
        P(TP),
        P(TP, None),
        P(TP),
        P("sp", None),
        P("sp", None),
        P("sp", None, TP),
        P("sp", None, TP),
        P("sp", None, TP),
        P(None, TP),
        P(None, TP),
        P(TP, None),
    )
    out_specs = P(TP, "sp")
    return jax.shard_map(local, mesh=split, in_specs=in_specs, out_specs=out_specs, check_vma=False)
```

time: 262 us -> 196 us (0.75)
  waiting for transfers between devices: 120 us -> 58.2 us
  blocking collectives: 67.2 us -> 35.8 us
  starting transfers between devices: 35.2 us -> 57.3 us
  local copies, waits for them, and re-layouts: 7.81 us -> 26.8 us
  between operations: 13.7 us -> 0.82 us
    all_gather x2 -> x0, waiting for transfers between devices: 86.5 us -> none  [the longest x1 48.8 us: local(): lax.all_gather(expert_mid, TP, axis=0, tiled=True)]
    all_to_all x2 -> x1, blocking collectives: 51.8 us -> 13.4 us  [sum_at_owner(): lax.all_to_all(pieces, axis, split_axis=0, concat_axis=0, tiled=True)]
    all_to_all x1, waiting for transfers between devices: 6.02 us -> 31 us  [from_everyone(): lax.all_to_all(jnp.broadcast_to(x[None], (size, *x.shape)), axis, 0, 0, t...]
    all_to_all x1 -> x2, starting transfers between devices: 14.4 us -> 29.5 us  [the longest x1 16.4 us: local(): lax.all_to_all(sent.reshape(sp_count, share * parts, feat_rows), 'sp', sp...]
    ppermute x2 -> x6, starting transfers between devices: 6.83 us -> 18.5 us  [shifted(): return lax.ppermute(x, axis, pairs)]
    slice x2 -> x8, local copies, waits for them, and re-layouts: 1.01 us -> 9.01 us  [the longest x5 8.05 us: part(): w = cycle[block][k][which].reshape(half, -1, feat_rows)]
    dot_general x6 -> x3, matrix products: 10.5 us -> 3.33 us  [contract_rows(): lax.dot_general(left, right, (((0,), (0,)), ((), ())), preferred_element_...]
    all_gather x1 -> x2, blocking collectives: 15.4 us -> 22.5 us  [the longest x1 12 us: local(): lax.all_gather(arrived.reshape(slot_total, parts * feat_rows), 'tx', axis=0)]
  transfers between devices with their start and end apart: 8 -> 10, of which waited for: 5 -> 5; matrix products, arithmetic and copies ran while one was open for 5% -> 13% of each run, Pallas kernels for 0% -> 0%
where the time goes in v1:
time: 196 us; the launch traced here: 194 us
  waiting for transfers between devices  58.2 us (30%)
  starting transfers between devices  57.3 us (29%)
  blocking collectives  35.8 us (18%)
  local copies, waits for them, and re-layouts  26.8 us (14%)
  matrix products  10.2 us (5%)
  other arithmetic  5.32 us (3%)
    all_to_all x1, waiting for transfers between devices, from_everyone(): lax.all_to_all(jnp.broadcast_to(x[None], (size, *x.shape)), axis, 0, 0, t...  31 us
    ppermute x6, starting transfers between devices, shifted(): return lax.ppermute(x, axis, pairs)  18.5 us
    all_to_all x1, waiting for transfers between devices, local(): lax.all_to_all(summed, 'sp', split_axis=0, concat_axis=0, tiled=True)  18.1 us
    all_to_all x1, starting transfers between devices, local(): lax.all_to_all(sent.reshape(sp_count, share * parts, feat_rows), 'sp', sp...  16.4 us
    all_to_all x1, blocking collectives, sum_at_owner(): lax.all_to_all(pieces, axis, split_axis=0, concat_axis=0, tiled=True)  13.4 us
    all_to_all x1, starting transfers between devices, local(): lax.all_to_all(summed, 'sp', split_axis=0, concat_axis=0, tiled=True)  13 us
    all_gather x1, blocking collectives, local(): lax.all_gather(arrived.reshape(slot_total, parts * feat_rows), 'tx', axis=0)  12 us
    all_gather x1, blocking collectives, local(): all_mid = lax.all_gather(expert_mid, 'tx', axis=0)  10.4 us
  transfers between devices with their start and end apart: 10, of which 5 were waited for; matrix products, arithmetic and copies ran while one was open for 13% of the time, Pallas kernels for 0%

profile of v1, /device:TPU:1, one launch (start us, length us, event | category | flops | bytes accessed | tf_op | source)
XLA Modules:
  0.0 194.5 jit_solution(6803149990213338296)
XLA Ops:
  0.0 0.9 slice.207
  0.9 0.8 slice.206
  1.8 4.9 %collective-permute-start = (bf16[2,64,2]{1,2,0:T(2,128)(2,1)S(1)}, bf16[2,64,2]{1,2,0:T(2,128)(2,1)S(1)}, u32[]{:S(2)}, u32[]{:S(2)}) collective-permute-start(bf16[2,64,2]{1,2,0:T(2,128)(2,1)S(1)} %pad_maximum_fusion.1), channel_id=1, source_target_pairs={{0,16},{16,32},{32,48},{48,64},{64,80},{80,96},{96,112},{112,128},... | collective-permute-start | bytes 1544 | tf_op jit(solution)/shard_map/ppermute | solution.py:18
  6.8 0.7 slice.211
  7.5 1.9 collective-permute-start.1
  9.4 0.8 slice_bitcast_fusion.4
  10.2 2.4 %collective-permute-done.1 = s32[2]{0:T(128)S(1)} collective-permute-done((s32[2]{0:T(128)S(1)}, s32[2]{0:T(128)S(1)}, u32[]{:S(2)}, u32[]{:S(2)}) %collective-permute-start.1) | collective-permute-done | bytes 40 | tf_op jit(solution)/shard_map/ppermute | solution.py:18
  12.6 0.7 pad_add_fusion
  13.4 0.7 compare_convert_fusion.2
  14.2 0.8 maximum_convert_fusion
  15.1 1.0 multiply_reduce_fusion.1
  16.1 1.4 fusion.2
  17.4 0.9 copy.181
  18.4 4.7 %all-to-all-start = ((bf16[16,128,128]{1,2,0:T(8,128)(2,1)}), bf16[16,128,128]{1,2,0:T(8,128)(2,1)S(1)}, u32[]{:S(2)}, u32[]{:S(2)}) async-start(bf16[16,128,128]{1,2,0:T(8,128)(2,1)} %bitcast.298), calls=%async_computation | async-start | bytes 1048576 | tf_op jit(solution)/shard_map/all_to_all | solution.py:23
  23.5 4.5 %collective-permute-start.2 = (bf16[2,3,1024,128]{3,2,1,0:T(8,128)(2,1)S(1)}, bf16[2,3,1024,128]{3,2,1,0:T(8,128)(2,1)}, u32[]{:S(2)}, u32[]{:S(2)}) collective-permute-start(bf16[2,3,1024,128]{3,2,1,0:T(8,128)(2,1)S(1)} %bitcast.299), channel_id=1, source_target_pairs={{0,12},{4,0},{8,4},{12,8},{1,13},{5,1},{9,5},{13,9},{2,14},{6,2},{... | collective-permute-start | bytes 4718600 | tf_op jit(solution)/shard_map/ppermute | solution.py:18
  27.9 1.9 collective-permute-start.3
  30.4 1.2 reduce-window.6
  32.1 1.8 all-to-all-done
  34.0 0.6 copy-done.9
  35.4 0.9 broadcast_in_dim.8
  36.3 4.7 %all-to-all-start.1 = ((bf16[16,144,128]{2,1,0:T(8,128)(2,1)}), bf16[16,144,128]{2,1,0:T(8,128)(2,1)S(1)}, u32[]{:S(2)}, u32[]{:S(2)}) async-start(bf16[16,144,128]{2,1,0:T(8,128)(2,1)} %broadcast_in_dim.8), calls=%async_computation.1 | async-start | bytes 1179648 | tf_op jit(solution)/shard_map/all_to_all | solution.py:29
  41.1 1.1 fusion.57
  42.1 31.0 %all-to-all-done.1 = bf16[16,144,128]{2,1,0:T(8,128)(2,1)S(1)} async-done(((bf16[16,144,128]{2,1,0:T(8,128)(2,1)}), bf16[16,144,128]{2,1,0:T(8,128)(2,1)S(1)}, u32[]{:S(2)}, u32[]{:S(2)}) %all-to-all-start.1) | async-done | bytes 589856 | tf_op jit(solution)/shard_map/all_to_all | solution.py:29
  73.6 0.8 reshape.206
  74.4 16.4 %all-to-all-start.2 = ((bf16[32,24,128]{2,1,0:T(8,128)(2,1)}), bf16[32,24,128]{2,1,0:T(8,128)(2,1)}, u32[]{:S(2)}, u32[]{:S(2)}) async-start(bf16[32,24,128]{2,1,0:T(8,128)(2,1)} %reshape.206), calls=%async_computation.2 | async-start | bytes 393216 | tf_op jit(solution)/shard_map/all_to_all | solution.py:145
  90.9 2.1 %slice_bitcast_fusion = bf16[3,1024,128]{2,1,0:T(8,128)(2,1)} fusion(bf16[2,3,1024,128]{3,2,1,0:T(8,128)(2,1)} %collective-permute-done.2), kind=kLoop, calls=%fused_computation.62 | loop fusion | bytes 1572864 | tf_op jit(solution)/shard_map/squeeze | solution.py:84
  93.0 2.1 %collective-permute-start.5 = (bf16[3,1024,128]{2,1,0:T(8,128)(2,1)}, bf16[3,1024,128]{2,1,0:T(8,128)(2,1)}, u32[]{:S(2)}, u32[]{:S(2)}) collective-permute-start(bf16[3,1024,128]{2,1,0:T(8,128)(2,1)} %slice_bitcast_fusion), channel_id=1, source_target_pairs={{0,12},{4,0},{8,4},{12,8},{1,13},{5,1},{9,5},{13,9},{2,14},{6,2},{... | collective-permute-start | bytes 2359304 | tf_op jit(solution)/shard_map/ppermute | solution.py:18
  95.0 2.1 %slice_bitcast_fusion.1 = bf16[3,1024,128]{2,1,0:T(8,128)(2,1)} fusion(bf16[2,3,1024,128]{3,2,1,0:T(8,128)(2,1)} %collective-permute-done.3), kind=kLoop, calls=%fused_computation.63 | loop fusion | bytes 1572864 | tf_op jit(solution)/shard_map/squeeze | solution.py:80
  97.1 3.2 %collective-permute-start.4 = (bf16[3,1024,128]{2,1,0:T(8,128)(2,1)}, bf16[3,1024,128]{2,1,0:T(8,128)(2,1)}, u32[]{:S(2)}, u32[]{:S(2)}) collective-permute-start(bf16[3,1024,128]{2,1,0:T(8,128)(2,1)} %slice_bitcast_fusion.1), channel_id=1, source_target_pairs={{0,4},{4,8},{8,12},{12,0},{1,5},{5,9},{9,13},{13,1},{2,6},{6,10},{... | collective-permute-start | bytes 2359304 | tf_op jit(solution)/shard_map/ppermute | solution.py:18
  100.3 2.3 %fusion.56 = (bf16[1,1,1024,128]{3,2,1,0:T(8,128)(2,1)S(1)}, bf16[1,1,1024,128]{3,2,1,0:T(8,128)(2,1)S(1)}, bf16[1,1,1024,128]{3,2,1,0:T(8,128)(2,1)}, bf16[1,1,...) fusion(bf16[2,3,1024,128]{3,2,1,0:T(8,128)(2,1)} %collective-permute-done.2), kind=kLoop, calls=%fused_computation.148 | loop fusion | bytes 3145728 | tf_op jit(solution)/shard_map/slice | solution.py:159
  102.7 2.3 %fusion.55 = (bf16[1,1,1024,128]{3,2,1,0:T(8,128)(2,1)S(1)}, bf16[1,1,1024,128]{3,2,1,0:T(8,128)(2,1)S(1)}, bf16[1,1,1024,128]{3,2,1,0:T(8,128)(2,1)}, bf16[1,1,...) fusion(bf16[2,3,1024,128]{3,2,1,0:T(8,128)(2,1)} %collective-permute-done.3), kind=kLoop, calls=%fused_computation.147 | loop fusion | bytes 3145728 | tf_op jit(solution)/shard_map/slice | solution.py:159
  105.0 4.8 %all-to-all-done.2 = bf16[32,24,128]{2,1,0:T(8,128)(2,1)} async-done(((bf16[32,24,128]{2,1,0:T(8,128)(2,1)}), bf16[32,24,128]{2,1,0:T(8,128)(2,1)}, u32[]{:S(2)}, u32[]{:S(2)}) %all-to-all-start.2) | async-done | bytes 196640 | tf_op jit(solution)/shard_map/all_to_all | solution.py:145
  109.7 1.7 all_gather_reshape.6
  111.4 12.0 %all_gather.6 = bf16[4,192,512]{2,1,0:T(8,128)(2,1)S(1)} all-gather(bf16[1,192,512]{2,1,0:T(8,128)(2,1)} %all_gather_reshape.6), channel_id=1, replica_groups=mesh['sp'=32,'ty'=4,'tx'=4] {'tx'}, dimensions={0}, use_global_device_ids=true | all-gather | bytes 983040 | tf_op jit(solution)/shard_map/all_gather | solution.py:169
  126.8 0.4 copy-done.5
  127.5 1.2 fusion.60
  129.1 1.2 fusion.59
  130.9 0.4 copy-done.18
  131.9 10.4 %all_gather.7 = bf16[4,192,512]{2,1,0:T(8,128)(2,1)S(1)} all-gather(bf16[1,192,512]{2,1,0:T(8,128)(2,1)S(1)} %all_gather_reshape.7), channel_id=1, replica_groups=mesh['sp'=32,'ty'=4,'tx'=4] {'tx'}, dimensions={0}, use_global_device_ids=true | all-gather | bytes 983040 | tf_op jit(solution)/shard_map/all_gather | solution.py:179
  144.6 0.8 copy.156
  145.4 13.0 %all-to-all-start.3 = ((bf16[32,24,128]{2,1,0:T(8,128)(2,1)}), bf16[32,24,128]{2,1,0:T(8,128)(2,1)S(1)}, u32[]{:S(2)}, u32[]{:S(2)}) async-start(bf16[32,24,128]{2,1,0:T(8,128)(2,1)} %bitcast.81), calls=%async_computation.3 | async-start | bytes 393216 | tf_op jit(solution)/shard_map/all_to_all | solution.py:184
  158.6 0.3 convolution_bitcast_fusion.26
  158.9 18.1 %all-to-all-done.3 = bf16[32,24,128]{2,1,0:T(8,128)(2,1)S(1)} async-done(((bf16[32,24,128]{2,1,0:T(8,128)(2,1)}), bf16[32,24,128]{2,1,0:T(8,128)(2,1)S(1)}, u32[]{:S(2)}, u32[]{:S(2)}) %all-to-all-start.3) | async-done | bytes 196640 | tf_op jit(solution)/shard_map/all_to_all | solution.py:184
  177.2 0.5 fusion.30
  178.0 0.4 mul.219
  178.5 1.6 fusion.3
  180.3 13.4 %all_to_all.25 = bf16[16,128,128]{1,2,0:T(8,128)(2,1)S(1)} all-to-all(bf16[16,128,128]{1,2,0:T(8,128)(2,1)S(1)} %bitcast.306), channel_id=1, replica_groups=mesh['sp'=32,'ty'=4,'tx'=4] {'ty','tx'}, dimensions={0} | all-to-all | bytes 1048576 | tf_op jit(solution)/shard_map/all_to_all | solution.py:23
  193.8 0.7 copy.161
  (132 shorter events, 11.1 us)
Async XLA Ops:
  0.0 178.5 %copy-start = (bf16[128,2048]{1,0:T(8,128)(2,1)S(1)}, bf16[128,2048]{1,0:T(8,128)(2,1)}, u32[]{:S(2)}) copy-start(bf16[128,2048]{1,0:T(8,128)(2,1)} %param.33) | copy-start | bytes 1572868
  1.8 12.2 %collective-permute-start = (bf16[2,64,2]{1,2,0:T(2,128)(2,1)S(1)}, bf16[2,64,2]{1,2,0:T(2,128)(2,1)S(1)}, u32[]{:S(2)}, u32[]{:S(2)}) collective-permute-start(bf16[2,64,2]{1,2,0:T(2,128)(2,1)S(1)} %pad_maximum_fusion.1), channel_id=1, source_target_pairs={{0,16},{16,32},{32,48},{48,64},{64,80},{80,96},{96,112},{112,128},... | collective-permute-start | bytes 1544 | tf_op jit(solution)/shard_map/ppermute | solution.py:18
  7.5 5.1 %collective-permute-start.1 = (s32[2]{0:T(128)S(1)}, s32[2]{0:T(128)S(1)}, u32[]{:S(2)}, u32[]{:S(2)}) collective-permute-start(s32[2]{0:T(128)S(1)} %slice.211), channel_id=1, source_target_pairs={{0,16},{16,32},{32,48},{48,64},{64,80},{80,96},{96,112},{112,128},... | collective-permute-start | bytes 32 | tf_op jit(solution)/shard_map/ppermute | solution.py:18
  15.1 8.0 %copy-start.12 = (bf16[1,2048,128]{2,1,0:T(8,128)(2,1)S(1)}, bf16[1,2048,128]{2,1,0:T(8,128)(2,1)}, u32[]{:S(2)}) copy-start(bf16[1,2048,128]{2,1,0:T(8,128)(2,1)} %param.30) | copy-start | bytes 1572868
  15.1 8.0 %copy-start.13 = (bf16[1,2048,128]{2,1,0:T(8,128)(2,1)S(1)}, bf16[1,2048,128]{2,1,0:T(8,128)(2,1)}, u32[]{:S(2)}) copy-start(bf16[1,2048,128]{2,1,0:T(8,128)(2,1)} %param.29) | copy-start | bytes 1572868
  15.1 8.0 %copy-start.14 = (bf16[1,2048,128]{2,1,0:T(8,128)(2,1)S(1)}, bf16[1,2048,128]{2,1,0:T(8,128)(2,1)}, u32[]{:S(2)}) copy-start(bf16[1,2048,128]{2,1,0:T(8,128)(2,1)} %param.28) | copy-start | bytes 1572868
  18.4 15.6 %all-to-all-start = ((bf16[16,128,128]{1,2,0:T(8,128)(2,1)}), bf16[16,128,128]{1,2,0:T(8,128)(2,1)S(1)}, u32[]{:S(2)}, u32[]{:S(2)}) async-start(bf16[16,128,128]{1,2,0:T(8,128)(2,1)} %bitcast.298), calls=%async_computation | async-start | bytes 1048576 | tf_op jit(solution)/shard_map/all_to_all | solution.py:23
  23.2 6.6 %copy-start.21 = (s32[128,4]{0,1:T(4,128)S(1)}, s32[128,4]{0,1:T(4,128)}, u32[]{:S(2)}) copy-start(s32[128,4]{0,1:T(4,128)} %param.26) | copy-start | bytes 6148
  23.3 7.0 %copy-start.20 = (bf16[128,128]{1,0:T(8,128)(2,1)S(1)}, bf16[128,128]{1,0:T(8,128)(2,1)}, u32[]{:S(2)}) copy-start(bf16[128,128]{1,0:T(8,128)(2,1)} %param.17) | copy-start | bytes 98308
  23.3 11.4 %copy-start.23 = (f32[128]{0:T(128)S(1)}, f32[128]{0:T(128)}, u32[]{:S(2)}) copy-start(f32[128]{0:T(128)} %param.25) | copy-start | bytes 1540
  23.5 67.4 %collective-permute-start.2 = (bf16[2,3,1024,128]{3,2,1,0:T(8,128)(2,1)S(1)}, bf16[2,3,1024,128]{3,2,1,0:T(8,128)(2,1)}, u32[]{:S(2)}, u32[]{:S(2)}) collective-permute-start(bf16[2,3,1024,128]{3,2,1,0:T(8,128)(2,1)S(1)} %bitcast.299), channel_id=1, source_target_pairs={{0,12},{4,0},{8,4},{12,8},{1,13},{5,1},{9,5},{13,9},{2,14},{6,2},{... | collective-permute-start | bytes 4718600 | tf_op jit(solution)/shard_map/ppermute | solution.py:18
  27.9 67.1 %collective-permute-start.3 = (bf16[2,3,1024,128]{3,2,1,0:T(8,128)(2,1)S(1)}, bf16[2,3,1024,128]{3,2,1,0:T(8,128)(2,1)}, u32[]{:S(2)}, u32[]{:S(2)}) collective-permute-start(bf16[2,3,1024,128]{3,2,1,0:T(8,128)(2,1)S(1)} %bitcast.300), channel_id=1, source_target_pairs={{0,4},{4,8},{8,12},{12,0},{1,5},{5,9},{9,13},{13,1},{2,6},{6,10},{... | collective-permute-start | bytes 4718600 | tf_op jit(solution)/shard_map/ppermute | solution.py:18
  30.4 6.0 %copy-start.15 = (bf16[128,128]{0,1:T(8,128)(2,1)}, bf16[128,128]{0,1:T(8,128)(2,1)S(1)}, u32[]{:S(2)}) copy-start(bf16[128,128]{0,1:T(8,128)(2,1)S(1)} %copy.136) | copy-start | bytes 98308
  34.0 0.6 copy-start.9
  36.3 36.9 %all-to-all-start.1 = ((bf16[16,144,128]{2,1,0:T(8,128)(2,1)}), bf16[16,144,128]{2,1,0:T(8,128)(2,1)S(1)}, u32[]{:S(2)}, u32[]{:S(2)}) async-start(bf16[16,144,128]{2,1,0:T(8,128)(2,1)} %broadcast_in_dim.8), calls=%async_computation.1 | async-start | bytes 1179648 | tf_op jit(solution)/shard_map/all_to_all | solution.py:29
  74.4 35.3 %all-to-all-start.2 = ((bf16[32,24,128]{2,1,0:T(8,128)(2,1)}), bf16[32,24,128]{2,1,0:T(8,128)(2,1)}, u32[]{:S(2)}, u32[]{:S(2)}) async-start(bf16[32,24,128]{2,1,0:T(8,128)(2,1)} %reshape.206), calls=%async_computation.2 | async-start | bytes 393216 | tf_op jit(solution)/shard_map/all_to_all | solution.py:145
  93.0 34.5 %collective-permute-start.5 = (bf16[3,1024,128]{2,1,0:T(8,128)(2,1)}, bf16[3,1024,128]{2,1,0:T(8,128)(2,1)}, u32[]{:S(2)}, u32[]{:S(2)}) collective-permute-start(bf16[3,1024,128]{2,1,0:T(8,128)(2,1)} %slice_bitcast_fusion), channel_id=1, source_target_pairs={{0,12},{4,0},{8,4},{12,8},{1,13},{5,1},{9,5},{13,9},{2,14},{6,2},{... | collective-permute-start | bytes 2359304 | tf_op jit(solution)/shard_map/ppermute | solution.py:18
  97.1 32.0 %collective-permute-start.4 = (bf16[3,1024,128]{2,1,0:T(8,128)(2,1)}, bf16[3,1024,128]{2,1,0:T(8,128)(2,1)}, u32[]{:S(2)}, u32[]{:S(2)}) collective-permute-start(bf16[3,1024,128]{2,1,0:T(8,128)(2,1)} %slice_bitcast_fusion.1), channel_id=1, source_target_pairs={{0,4},{4,8},{8,12},{12,0},{1,5},{5,9},{9,13},{13,1},{2,6},{6,10},{... | collective-permute-start | bytes 2359304 | tf_op jit(solution)/shard_map/ppermute | solution.py:18
  102.7 20.8 %copy-start.4 = (bf16[1,1,2,4,128,128]{5,4,3,2,1,0:T(8,128)(2,1)S(1)}, bf16[1,1,2,4,128,128]{5,4,3,2,1,0:T(8,128)(2,1)}, u32[]{:S(2)}) copy-start(bf16[1,1,2,4,128,128]{5,4,3,2,1,0:T(8,128)(2,1)} %get-tuple-element.27) | copy-start | bytes 786436
  105.0 18.8 %copy-start.3 = (bf16[1,1,2,4,128,128]{5,4,3,2,1,0:T(8,128)(2,1)S(1)}, bf16[1,1,2,4,128,128]{5,4,3,2,1,0:T(8,128)(2,1)}, u32[]{:S(2)}) copy-start(bf16[1,1,2,4,128,128]{5,4,3,2,1,0:T(8,128)(2,1)} %get-tuple-element.29) | copy-start | bytes 786436
  111.4 12.6 %copy-start.8 = (bf16[1,1,1024,128]{3,2,1,0:T(8,128)(2,1)S(1)}, bf16[1,1,1024,128]{3,2,1,0:T(8,128)(2,1)}, u32[]{:S(2)}) copy-start(bf16[1,1,1024,128]{3,2,1,0:T(8,128)(2,1)} %get-tuple-element.23) | copy-start | bytes 786436
  123.5 1.0 copy-start.7
  123.8 1.0 copy-start.1
  124.5 1.0 copy-start.17
  125.0 1.0 copy-start.6
  125.3 1.0 copy-start.19
  126.2 1.0 copy-start.5
  130.3 1.0 copy-start.18
  131.5 10.8 %copy-start.2 = (bf16[1,1,2,4,128,128]{5,4,3,2,1,0:T(8,128)(2,1)S(1)}, bf16[1,1,2,4,128,128]{5,4,3,2,1,0:T(8,128)(2,1)}, u32[]{:S(2)}) copy-start(bf16[1,1,2,4,128,128]{5,4,3,2,1,0:T(8,128)(2,1)} %get-tuple-element.26) | copy-start | bytes 786436
  144.2 14.3 %copy-start.22 = (f32[128,4]{0,1:T(4,128)S(1)}, f32[128,4]{0,1:T(4,128)}, u32[]{:S(2)}) copy-start(f32[128,4]{0,1:T(4,128)} %param.27) | copy-start | bytes 6148
  144.2 14.3 %copy-start.11 = (bf16[2048,128]{1,0:T(8,128)(2,1)S(1)}, bf16[2048,128]{1,0:T(8,128)(2,1)}, u32[]{:S(2)}) copy-start(bf16[2048,128]{1,0:T(8,128)(2,1)} %param.31) | copy-start | bytes 1572868
  145.4 31.6 %all-to-all-start.3 = ((bf16[32,24,128]{2,1,0:T(8,128)(2,1)}), bf16[32,24,128]{2,1,0:T(8,128)(2,1)S(1)}, u32[]{:S(2)}, u32[]{:S(2)}) async-start(bf16[32,24,128]{2,1,0:T(8,128)(2,1)} %bitcast.81), calls=%async_computation.3 | async-start | bytes 393216 | tf_op jit(solution)/shard_map/all_to_all | solution.py:184
  180.1 13.6 %copy-start.10 = (f32[128,128]{0,1:T(8,128)S(1)}, f32[128,128]{0,1:T(8,128)}, u32[]{:S(2)}) copy-start(f32[128,128]{0,1:T(8,128)} %copy-done.9) | copy-start | bytes 196612
  180.1 13.6 %copy-start.16 = (bf16[128,128]{0,1:T(8,128)(2,1)S(1)}, bf16[128,128]{0,1:T(8,128)(2,1)}, u32[]{:S(2)}) copy-start(bf16[128,128]{0,1:T(8,128)(2,1)} %copy-done.15) | copy-start | bytes 98308
